TPU v7x, 32 devices: a whole 2x2x4 slice. The times are simulated.
32 devices in a mesh: sp: 8 (over z, x), tp: 4 (over y, core).
Axes of the slice: x: 2, y: 2, z: 4, core: 2. Of those that a mesh axis runs over, the one named last changes fastest.
Arguments:
- tokens: bfloat16 [4096, 2048], P('sp', 'tp'), may hold values from -6 to 6
- norm_gain: float32 [2048], replicated, may hold values from 0.1 to 1.9
- proj_state: bfloat16 [2048, 1024], P('sp', 'tp'), may hold values from -0.125 to 0.125
- proj_value: bfloat16 [2048, 1024], P('sp', 'tp'), may hold values from -0.125 to 0.125
- proj_gate: bfloat16 [2048, 1024], P('sp', 'tp'), may hold values from -0.125 to 0.125
- eigen_real: float32 [64, 64], P('tp')
- eigen_imag: float32 [64, 64], P('tp')
- log_step: float32 [64], P('tp')
- decay_shift: float32 [64, 4096], P('tp', 'sp'), may hold values from -2.2 to 0
- state_input: float32 [2, 64, 16, 64], P(None, 'tp'), may hold values from -1 to 1
- state_readout_matrices: float32 [2, 64, 16, 64], P(None, 'tp'), may hold values from -0.5 to 0.5
- skip_gain: float32 [1024], P('tp'), may hold values from -5 to 5
- init_state: float32 [2, 64, 64], P(None, 'tp'), may hold values from -5 to 5
- conv_taps: float32 [31, 1024], P(None, 'tp')
- channel_gain: float32 [1024], P('tp'), may hold values from 0.1 to 1.9
- merge_state: bfloat16 [1024, 2048], P('tp', 'sp'), may hold values from -0.125 to 0.125
- merge_conv: bfloat16 [1024, 2048], P('tp', 'sp'), may hold values from -0.125 to 0.125
Outputs:
- mixed: bfloat16 [4096, 2048], P(('sp', 'tp'))
All inputs are finite; a program needn't handle non-finite values.
Results may differ from a plain program's by a relative error of at most 0.011.
Values may be sent and summed in bfloat16 or wider, within the bound.
A program may use at most 128 MiB of HBM per device.

v0:
```python
import functools

import jax
import jax.numpy as jnp
from jax import lax
from jax.experimental import pallas as pl
from jax.experimental.pallas import tpu as pltpu
from jax.sharding import PartitionSpec as P

CONV_W = 1024


epsilon = 1e-06
exact_precision = lax.Precision.HIGHEST


def entering(value, axis, join, neutral):
    count, mine = (lax.axis_size(axis), lax.axis_index(axis))
    pieces = jax.tree.map(lambda part: lax.all_gather(part, axis), value)
    total = jax.tree.map(
        lambda part, zero: jnp.full_like(part, 0) + jnp.asarray(zero, part.dtype), value, neutral
    )

    def hop(position, total):
        longer = join(total, jax.tree.map(lambda part: part[position], pieces))
        return jax.tree.map(lambda new, old: jnp.where(position < mine, new, old), longer, total)

    return lax.fori_loop(0, count - 1, hop, total)


def passed_along(block, axis, distance):
    devices = range(lax.axis_size(axis))
    route = [(i - distance, i) for i in devices if i - distance in devices]
    return lax.ppermute(block, axis, route)


def round_half(value):
    return lax.optimization_barrier(value.astype(jnp.bfloat16))


def input_matrix(eigen_real, eigen_imag, step, state_input):
    base = eigen_real * step[:, None]
    theta = eigen_imag * step[:, None]
    magnitude = jnp.exp(base)
    near_re = magnitude * jnp.cos(theta) - 1.0
    near_im = magnitude * jnp.sin(theta)
    modulus = eigen_real * eigen_real + eigen_imag * eigen_imag
    ratio_re = (near_re * eigen_real + near_im * eigen_imag) / modulus
    ratio_im = (near_im * eigen_real - near_re * eigen_imag) / modulus
    in_re = state_input[0]
    in_im = state_input[1]
    discrete_decay_real = ratio_re[:, None, :] * in_re - ratio_im[:, None, :] * in_im
    discrete_decay_imaginary = ratio_re[:, None, :] * in_im + ratio_im[:, None, :] * in_re
    return (discrete_decay_real, discrete_decay_imaginary)


def block_states(c_re, c_im, delta_real, delta_imaginary, shift, base, theta, counts, lower):
    level = jnp.cumsum(shift, axis=0)[:, :, None] + counts * base
    angle = counts * theta
    cosine = jnp.cos(angle)
    sine = jnp.sin(angle)
    grow = jnp.exp(level)
    shrink = jnp.exp(-level)
    w_re = shrink * (cosine * delta_real + sine * delta_imaginary)
    w_im = shrink * (cosine * delta_imaginary - sine * delta_real)
    length, groups, states = delta_real.shape
    stacked = jnp.concatenate([w_re, w_im], axis=1).reshape(length, 2 * groups * states)
    summed = jnp.dot(lower, stacked, precision=exact_precision).reshape(length, 2 * groups, states)
    t_re = summed[:, :groups] + c_re
    t_im = summed[:, groups:] + c_im
    input_real = grow * (cosine * t_re - sine * t_im)
    input_imaginary = grow * (cosine * t_im + sine * t_re)
    return (input_real, input_imaginary)


def chain(earlier, later):
    a_re, a_im, b_re, b_im = earlier
    c_re, c_im, delta_real, delta_imaginary = later
    return (
        a_re * c_re - a_im * c_im,
        a_re * c_im + a_im * c_re,
        c_re * b_re - c_im * b_im + delta_real,
        c_re * b_im + c_im * b_re + delta_imaginary,
    )


def state_local(
    u_in, eigen_real, eigen_imag, log_step, decay_shift, state_input, state_readout_matrices
):
    count, width = u_in.shape
    groups, states = eigen_real.shape
    group = width // groups
    step = jnp.exp(log_step)
    base = eigen_real * step[:, None]
    theta = eigen_imag * step[:, None]
    discrete_decay_real, discrete_decay_imaginary = input_matrix(
        eigen_real, eigen_imag, step, state_input
    )
    float_values = u_in.astype(jnp.float32).reshape(count, groups, group)
    forcing_real = jnp.einsum(
        "ovi,viu->ovu", float_values, discrete_decay_real, precision=exact_precision
    )
    forcing_imaginary = jnp.einsum(
        "ovi,viu->ovu", float_values, discrete_decay_imaginary, precision=exact_precision
    )
    shift = decay_shift.T
    length = min(32, count)
    blocks = count // length
    counts = (jnp.arange(length) + 1).astype(jnp.float32)[:, None, None]
    lower = (jnp.arange(length)[:, None] >= jnp.arange(length)[None, :]).astype(jnp.float32)

    def advance(carry, inputs):
        delta_real, delta_imaginary, block_shift = inputs
        input_real, input_imaginary = block_states(
            carry[0], carry[1], delta_real, delta_imaginary, block_shift, base, theta, counts, lower
        )
        return ((input_real[-1], input_imaginary[-1]), (input_real, input_imaginary))

    zero = jnp.zeros((groups, states), jnp.float32)
    last, (input_real, input_imaginary) = lax.scan(
        advance,
        (zero, zero),
        (
            forcing_real.reshape(blocks, length, groups, states),
            forcing_imaginary.reshape(blocks, length, groups, states),
            shift.reshape(blocks, length, groups),
        ),
    )
    input_real = input_real.reshape(count, groups, states)
    input_imaginary = input_imaginary.reshape(count, groups, states)
    local_output = jnp.einsum(
        "lan,arn->lar", input_real, state_readout_matrices[0], precision=exact_precision
    ) - jnp.einsum(
        "lan,arn->lar", input_imaginary, state_readout_matrices[1], precision=exact_precision
    )
    whole_count = (jnp.arange(count) + 1).astype(jnp.float32)[:, None, None]
    level = jnp.cumsum(shift, axis=0)[:, :, None] + whole_count * base
    angle = whole_count * theta
    grow = jnp.exp(level)
    exponent_real = grow * jnp.cos(angle)
    exponent_imaginary = grow * jnp.sin(angle)
    summary = (exponent_real[-1], exponent_imaginary[-1], last[0], last[1])
    return (local_output, exponent_real, exponent_imaginary, summary)


def carry_in(summary, init_state):
    groups, states = summary[0].shape
    ones = jnp.ones((groups, states), jnp.float32)
    zeros = jnp.zeros((groups, states), jnp.float32)
    identity = (ones, zeros, zeros, zeros)
    before = entering(summary, "sp", chain, identity)
    a_re, a_im, b_re, b_im = before
    s_re = init_state[0]
    s_im = init_state[1]
    return (a_re * s_re - a_im * s_im + b_re, a_re * s_im + a_im * s_re + b_im)


def state_finish(
    local_output,
    exponent_real,
    exponent_imaginary,
    carried,
    state_readout_matrices,
    skip_gain,
    u_in,
):
    h_re, h_im = carried
    output_real = state_readout_matrices[0]
    output_imaginary = state_readout_matrices[1]
    blend_real = output_real * h_re[:, None, :] - output_imaginary * h_im[:, None, :]
    blend_imaginary = output_real * h_im[:, None, :] + output_imaginary * h_re[:, None, :]
    total = (
        local_output
        + jnp.einsum("lan,arn->lar", exponent_real, blend_real, precision=exact_precision)
        - jnp.einsum("lan,arn->lar", exponent_imaginary, blend_imaginary, precision=exact_precision)
    )
    count, width = u_in.shape
    groups = local_output.shape[1]
    float_values = u_in.astype(jnp.float32).reshape(count, groups, width // groups)
    total = total + skip_gain.reshape(groups, width // groups) * float_values
    return jax.nn.gelu(total).reshape(count, width).astype(jnp.bfloat16)


def conv_branch(value, gate, conv_taps, channel_gain):
    glu = round_half(value.astype(jnp.float32) * jax.nn.sigmoid(gate.astype(jnp.float32)))
    reach = conv_taps.shape[0] - 1
    count = glu.shape[0]
    before = passed_along(glu[count - reach :], "sp", 1)
    extended = jnp.concatenate([before, glu], axis=0).astype(jnp.float32)
    raw = jnp.zeros(glu.shape, jnp.float32)
    for offset in range(reach + 1):
        raw = raw + conv_taps[offset] * extended[offset : offset + count]
    first, second = lax.psum(
        (jnp.sum(raw, axis=1, keepdims=True), jnp.sum(raw * raw, axis=1, keepdims=True)), "tp"
    )
    middle = first / CONV_W
    spread = second / CONV_W - middle * middle
    scaled = (raw - middle) * lax.rsqrt(spread + epsilon) * channel_gain
    return jax.nn.silu(scaled).astype(jnp.bfloat16)


def per_device(
    tokens,
    norm_gain,
    proj_state,
    proj_value,
    proj_gate,
    eigen_real,
    eigen_imag,
    log_step,
    decay_shift,
    state_input,
    state_readout_matrices,
    skip_gain,
    init_state,
    conv_taps,
    channel_gain,
    merge_state,
    merge_conv,
):
    whole = lax.all_gather(tokens, "tp", axis=1, tiled=True)
    wide = whole.astype(jnp.float32)
    normed = (
        wide * lax.rsqrt(jnp.mean(wide * wide, axis=1, keepdims=True) + epsilon) * norm_gain
    ).astype(jnp.bfloat16)
    pieces = (
        lax.all_gather(proj_state, "sp", axis=0, tiled=True),
        lax.all_gather(proj_value, "sp", axis=0, tiled=True),
        lax.all_gather(proj_gate, "sp", axis=0, tiled=True),
    )
    state_sum, value_sum, gate_sum = tuple(
        (jnp.dot(normed, piece, preferred_element_type=jnp.float32) for piece in pieces)
    )
    u_in = round_half(state_sum)
    local_output, exponent_real, exponent_imaginary, summary = state_local(
        u_in, eigen_real, eigen_imag, log_step, decay_shift, state_input, state_readout_matrices
    )
    carried = carry_in(summary, init_state)
    conv_out = conv_branch(round_half(value_sum), round_half(gate_sum), conv_taps, channel_gain)
    ssm_out = state_finish(
        local_output,
        exponent_real,
        exponent_imaginary,
        carried,
        state_readout_matrices,
        skip_gain,
        u_in,
    )
    full_state, full_conv = (
        lax.all_gather(merge_state, "sp", axis=1, tiled=True),
        lax.all_gather(merge_conv, "sp", axis=1, tiled=True),
    )
    return lax.psum_scatter(
        (
            jnp.dot(ssm_out, full_state, preferred_element_type=jnp.float32)
            + jnp.dot(conv_out, full_conv, preferred_element_type=jnp.float32)
        ).astype(jnp.bfloat16),
        "tp",
        scatter_dimension=0,
        tiled=True,
    )


MESH = pl.DeviceIdType.MESH
F32 = jnp.float32
BF16 = jnp.bfloat16
BLOCK = 32


def dot(a, b):
    return jnp.dot(a, b, preferred_element_type=F32)


def dot_exact(a, b):
    return jnp.dot(a, b, preferred_element_type=F32, precision=exact_precision)


def split(value):
    high = value.astype(BF16)
    return high, (value - high.astype(F32)).astype(BF16)


def ring_position(index, n):
    return jnp.where(index % 2 == 0, index // 2, n - 1 - index // 2)


def ring_index(position, n):
    position = lax.rem(position + 2 * n, n)
    return jnp.where(position < n // 2, 2 * position, 2 * (n - 1 - position) + 1)


def mixer_kernel(
    n, ntp,
    tokens, gain, proj_s, proj_v, proj_g, shift, expand, base_t, cos_t, sin_t,
    binp, cout, skip, init, taps, chgain, merge_s, merge_c,
    out,
    tok, normed, gat, mgat, u_buf, forc, grow_buf, xs, ext, raw, ssm, conv,
    halo, glu_tail, summ, summ_in, stat, stat_in, snd, own, rp, s2, r2,
    loc_sem, tok_s, tok_r, fwd_s, fwd_r, ring_s, ring_r, halo_s, halo_r,
    sum_s, sum_r, st_s, st_r, rp_s, rp_r, r2_s, r2_r,
):
    sp = lax.axis_index("sp")
    tp = lax.axis_index("tp")
    ny = ntp // 2
    y, core = tp // 2, tp % 2
    partner = y * 2 + 1 - core
    pos = ring_position(sp, n)
    right, left = ring_index(pos + 1, n), ring_index(pos - 1, n)
    count, width = u_buf.shape
    lanes = grow_buf.shape[1]
    part = tokens.shape[1]
    rows_w = proj_s.shape[0]

    halo[...] = jnp.zeros_like(halo)
    summ_in[...] = jnp.zeros_like(summ_in)

    barrier = pltpu.get_barrier_semaphore()
    for d in range(1, n):
        pl.semaphore_signal(barrier, inc=1, device_id=(lax.rem(sp + d, n), tp), device_id_type=MESH)
    for d in range(1, ntp):
        pl.semaphore_signal(barrier, inc=1, device_id=(sp, lax.rem(tp + d, ntp)), device_id_type=MESH)
    pl.semaphore_wait(barrier, n + ntp - 2)

    def remote(src, dst, s, r, where):
        return pltpu.make_async_remote_copy(
            src_ref=src, dst_ref=dst, send_sem=s, recv_sem=r, device_id=where, device_id_type=MESH
        )

    sources = (proj_s, proj_v, proj_g, merge_s, merge_c)
    hops = n // 2

    def slot(w, origin):
        return gat.at[w, origin] if w < 3 else mgat.at[w - 3, origin]

    def piece(w, side, step):
        origin = ring_index(pos - step if side == 0 else pos + step, n)
        where = (right if side == 0 else left, tp)
        src = sources[w] if step == 0 else slot(w, origin)
        dst = slot(w, origin)
        if step == hops - 1:
            half = src.shape[0] // 2
            window = pl.ds(side * half, half)
            src, dst = src.at[window], dst.at[window]
        return remote(src, dst, ring_s.at[w, side, step], ring_r.at[w, side, step], where)

    def ring_send(ws, step):
        for w in ws:
            for side in range(2):
                if step > 0:
                    piece(w, side, step - 1).wait_recv()
                piece(w, side, step).start()

    def ring_end(ws):
        for w in ws:
            for side in range(2):
                piece(w, side, hops - 1).wait_recv()

    proj_set, merge_set = range(3), range(3, 5)
    ring_send(proj_set, 0)

    def tok_copy(d):
        where = (sp, lax.rem(y + d, ny) * 2 + core) if d else (sp, partner)
        return remote(tokens, tok.at[tp], tok_s.at[d], tok_r.at[d], where)

    def tok_forward(d):
        origin = lax.rem(y - d + ny, ny) * 2 + core
        return remote(tok.at[origin], tok.at[origin], fwd_s.at[d], fwd_r.at[d], (sp, partner))

    for d in list(range(1, ny)) + [0]:
        tok_copy(d).start()
    local = [pltpu.make_async_copy(tokens, tok.at[tp], loc_sem.at[5])]
    for w in range(5):
        local.append(pltpu.make_async_copy(sources[w], slot(w, sp), loc_sem.at[w]))
    for c in local:
        c.start()
    ring_send(proj_set, 1)
    for d in range(1, ny):
        tok_copy(d).wait_recv()
        tok_forward(d).start()
    tok_copy(0).wait_recv()
    for c in local:
        c.wait()
    for step in range(2, hops - 1):
        ring_send(proj_set, step)
    for d in range(1, ny):
        tok_forward(d).wait_recv()

    tile = 64

    @pl.loop(0, count // tile)
    def _(i):
        rows = pl.ds(pl.multiple_of(i * tile, tile), tile)
        pieces = [tok[j, rows, :].astype(F32) for j in range(ntp)]
        square = sum(jnp.sum(p * p, axis=1, keepdims=True) for p in pieces)
        scale = lax.rsqrt(square / (part * ntp) + epsilon)
        for j in range(ntp):
            cols = slice(j * part, (j + 1) * part)
            normed[rows, cols] = (pieces[j] * scale * gain[:, cols]).astype(BF16)

    ring_send(proj_set, hops - 1)
    ring_send(merge_set, 0)
    ring_end(proj_set)

    big = 128

    def project(w, i):
        rows = pl.ds(pl.multiple_of(i * big, big), big)
        total = dot(normed[rows, 0:rows_w], gat[w, 0])
        for o in range(1, n):
            total += dot(normed[rows, o * rows_w : (o + 1) * rows_w], gat[w, o])
        return rows, total.astype(BF16)

    @pl.loop(0, count // big)
    def _(i):
        rows, value = project(1, i)
        rows, gate = project(2, i)
        glu = (value.astype(F32) * jax.nn.sigmoid(gate.astype(F32))).astype(BF16)
        ext[pl.ds(pl.multiple_of(BLOCK + i * big, BLOCK), big), :] = glu.astype(F32)
        rows, u = project(0, i)
        u_buf[rows, :] = u

    ring_send(merge_set, 1)
    glu_tail[...] = ext[count : count + BLOCK, :].astype(BF16)
    halo_to = lax.rem(sp + 1, n)
    halo_copy = remote(glu_tail, halo, halo_s, halo_r, (halo_to, tp))

    @pl.when(sp < n - 1)
    def _():
        halo_copy.start()

    wide = 256

    @pl.loop(0, 2 * lanes // wide)
    def _(j):
        cols = pl.ds(pl.multiple_of(j * wide, wide), wide)
        high, low = split(binp[:, cols])
        forc[:, cols] = dot(u_buf[...], high) + dot(u_buf[...], low)

    row_i = lax.broadcasted_iota(jnp.int32, (BLOCK, BLOCK), 0)
    col_i = lax.broadcasted_iota(jnp.int32, (BLOCK, BLOCK), 1)
    lower = (row_i >= col_i).astype(F32)
    last = slice(BLOCK - 1, BLOCK)

    def first_pass(k, state):
        a_re, a_im, c_re, c_im = state
        rows = pl.ds(pl.multiple_of(k * BLOCK, BLOCK), BLOCK)
        level = dot_exact(dot_exact(lower, shift[rows, :]), expand[...]) + base_t[...]
        grow, shrink = jnp.exp(level), jnp.exp(-level)
        cosine, sine = cos_t[...], sin_t[...]
        d_re, d_im = forc[rows, :lanes], forc[rows, lanes:]
        w_re = shrink * (cosine * d_re + sine * d_im)
        w_im = shrink * (cosine * d_im - sine * d_re)
        forc[rows, :lanes] = w_re
        forc[rows, lanes:] = w_im
        grow_buf[rows, :] = grow
        e_re, e_im = grow[last] * cosine[last], grow[last] * sine[last]
        t_re = c_re + jnp.sum(w_re, axis=0, keepdims=True)
        t_im = c_im + jnp.sum(w_im, axis=0, keepdims=True)
        return (
            a_re * e_re - a_im * e_im,
            a_re * e_im + a_im * e_re,
            e_re * t_re - e_im * t_im,
            e_re * t_im + e_im * t_re,
        )

    zero = jnp.zeros((1, lanes), F32)
    ended = lax.fori_loop(0, count // BLOCK, first_pass, (zero + 1.0, zero, zero, zero))
    half = lanes // 2
    for r in range(4):
        summ[r : r + 1, :] = ended[r][:, :half]
        summ[4 + r : 5 + r, :] = ended[r][:, half:]

    def summ_copy(d):
        return remote(summ, summ_in.at[sp], sum_s.at[d], sum_r.at[d], (lax.rem(sp + d, n), tp))

    for d in range(1, n):

        @pl.when(sp + d < n)
        def _():
            summ_copy(d).start()

    ring_send(merge_set, 2) if hops > 2 else None

    @pl.when(sp > 0)
    def _():
        halo_copy.wait_recv()

    ext[0:BLOCK, :] = halo[...].astype(F32)
    reach = taps.shape[0] - 1

    @pl.loop(0, count // tile)
    def _(i):
        start = pl.multiple_of(i * tile, tile)
        window = ext[pl.ds(start, tile + BLOCK), :]
        total = jnp.zeros((tile, width), F32)
        for k in range(reach + 1):
            at = BLOCK - reach + k
            total += taps[k : k + 1, :] * window[at : at + tile, :]
        raw[pl.ds(start, tile), :] = total

    lane = lax.broadcasted_iota(jnp.int32, (count, 128), 1)
    values = raw[...]
    first = jnp.sum(values, axis=1, keepdims=True)
    second = jnp.sum(values * values, axis=1, keepdims=True)
    packed = jnp.where(lane == 0, first, jnp.where(lane == 1, second, 0.0))
    stat[...] = packed.T[0:8, :]

    def stat_copy(d):
        return remote(stat, stat_in.at[d], st_s.at[d], st_r.at[d], (sp, lax.rem(tp + d, ntp)))

    for d in range(1, ntp):
        stat_copy(d).start()
    for step in range(3, hops):
        ring_send(merge_set, step)

    for d in range(1, n):

        @pl.when(sp >= d)
        def _():
            summ_copy(d).wait_recv()

    def unpack(block):
        return [jnp.concatenate([block[r : r + 1], block[4 + r : 5 + r]], axis=1) for r in range(4)]

    h_re, h_im = init[0:1, :], init[1:2, :]
    for q in range(n - 1):
        a_re, a_im, b_re, b_im = unpack(summ_in[q])
        n_re = a_re * h_re - a_im * h_im + b_re
        n_im = a_re * h_im + a_im * h_re + b_im
        h_re = jnp.where(q < sp, n_re, h_re)
        h_im = jnp.where(q < sp, n_im, h_im)

    lower_half = lower.astype(BF16)

    def second_pass(k, state):
        c_re, c_im = state
        rows = pl.ds(pl.multiple_of(k * BLOCK, BLOCK), BLOCK)
        high, low = split(forc[rows, :])
        summed = dot(lower_half, high) + dot(lower_half, low)
        t_re = summed[:, :lanes] + c_re
        t_im = summed[:, lanes:] + c_im
        grow = grow_buf[rows, :]
        g_re, g_im = grow * cos_t[...], grow * sin_t[...]
        x_re = g_re * t_re - g_im * t_im
        x_im = g_re * t_im + g_im * t_re
        xs[rows, :lanes] = x_re.astype(BF16)
        xs[rows, lanes:] = x_im.astype(BF16)
        return x_re[last], x_im[last]

    lax.fori_loop(0, count // BLOCK, second_pass, (h_re, h_im))

    @pl.loop(0, count // big)
    def _(i):
        rows = pl.ds(pl.multiple_of(i * big, big), big)
        total = dot(xs[rows, :], cout[...])
        total += skip[...] * u_buf[rows, :].astype(F32)
        ssm[rows, :] = jax.nn.gelu(total).astype(BF16)

    for d in range(1, ntp):
        stat_copy(d).wait_recv()
    sums = stat[...]
    for d in range(1, ntp):
        sums += stat_in[d]
    channels = width * ntp
    middle_row = sums[0:1] / channels
    inverse_row = lax.rsqrt(sums[1:2] / channels - middle_row * middle_row + epsilon)
    row = lax.broadcasted_iota(jnp.int32, (128, count), 0)
    columns = jnp.where(row == 0, middle_row, inverse_row).T
    scaled = (raw[...] - columns[:, 0:1]) * columns[:, 1:2] * chgain[...]
    conv[...] = jax.nn.silu(scaled).astype(BF16)

    ring_end(merge_set)
    quarters, block_rows = snd.shape[1], snd.shape[2]
    per = n // quarters
    cw = merge_s.shape[1]

    def product(block, q):
        rows = pl.ds(pl.multiple_of(block * block_rows, block_rows), block_rows)
        a, b = ssm[rows, :], conv[rows, :]
        outs = []
        for o in range(q * per, (q + 1) * per):
            outs.append((dot(a, mgat[0, o]) + dot(b, mgat[1, o])).astype(BF16))
        return outs

    def to_partner(d, q):
        return remote(snd.at[d, q], rp.at[d, q], rp_s.at[d, q], rp_r.at[d, q], (sp, partner))

    def across(d, q):
        where = (sp, lax.rem(y + d, ny) * 2 + core)
        return remote(s2.at[d, q], r2.at[d, q], r2_s.at[d, q], r2_r.at[d, q], where)

    order = list(range(1, ny)) + [0]

    def fill(buffer, d, q, which):
        for i, value in enumerate(product(lax.rem(y + d, ny) * 2 + which, q)):
            buffer[d, q, :, i * cw : (i + 1) * cw] = value

    def relay(d, q):
        to_partner(d, q).wait_recv()
        s2[d, q] = (own[d, q].astype(F32) + rp[d, q].astype(F32)).astype(BF16)
        across(d, q).start()

    for d in order:
        for q in range(quarters):
            fill(snd, d, q, 1 - core)
            to_partner(d, q).start()
            fill(own, d, q, core)
            if d and q:
                relay(d, q - 1)
        if d:
            relay(d, quarters - 1)
    for q in range(quarters):
        to_partner(0, q).wait_recv()
        total = own[0, q].astype(F32) + rp[0, q].astype(F32)
        for d in range(1, ny):
            across(d, q).wait_recv()
            total += r2[d, q].astype(F32)
        out[:, q * per * cw : (q + 1) * per * cw] = total.astype(BF16)

    for w in range(5):
        for side in range(2):
            for step in range(hops):
                piece(w, side, step).wait_send()
    for d in range(ny):
        tok_copy(d).wait_send()
        if d:
            tok_forward(d).wait_send()
        for q in range(quarters):
            to_partner(d, q).wait_send()
            if d:
                across(d, q).wait_send()
    for d in range(1, ntp):
        stat_copy(d).wait_send()

    @pl.when(sp < n - 1)
    def _():
        halo_copy.wait_send()

    for d in range(1, n):

        @pl.when(sp + d < n)
        def _():
            summ_copy(d).wait_send()


def fused(
    n, ntp, tokens, norm_gain, proj_state, proj_value, proj_gate, eigen_real, eigen_imag,
    log_step, decay_shift, state_input, state_readout_matrices, skip_gain, init_state,
    conv_taps, channel_gain, merge_state, merge_conv,
):
    count, part = tokens.shape
    groups, states = eigen_real.shape
    width = proj_state.shape[1]
    lanes = groups * states
    features = part * ntp
    step = jnp.exp(log_step)
    base = (eigen_real * step[:, None]).reshape(1, lanes)
    theta = (eigen_imag * step[:, None]).reshape(1, lanes)
    counts = (jnp.arange(BLOCK) + 1).astype(F32)[:, None]
    angle = counts * theta
    b_re, b_im = input_matrix(eigen_real, eigen_imag, step, state_input)
    group = width // groups
    same = jnp.arange(width)[:, None] // group == jnp.arange(lanes)[None, :] // states

    def spread_out(matrix):
        tiled = jnp.tile(matrix.reshape(width, states), (1, groups))
        return jnp.where(same, tiled, 0.0)

    binp = jnp.concatenate([spread_out(b_re), spread_out(b_im)], axis=1)
    cout = jnp.concatenate(
        [spread_out(state_readout_matrices[0]), -spread_out(state_readout_matrices[1])], axis=1
    ).astype(BF16).T
    expand = (jnp.arange(groups)[:, None] == jnp.arange(lanes)[None, :] // states).astype(F32)
    quarters = min(4, n)
    ny = ntp // 2
    block_rows = count // ntp
    cw = merge_state.shape[1] * n // quarters
    pieces = pltpu.VMEM((ny, quarters, block_rows, cw), BF16)
    vmem = pl.BlockSpec(memory_space=pltpu.VMEM)
    hops = n // 2
    dma = pltpu.SemaphoreType.DMA
    return pl.pallas_call(
        functools.partial(mixer_kernel, n, ntp),
        out_shape=jax.ShapeDtypeStruct((block_rows, features), BF16),
        in_specs=[vmem] * 18,
        out_specs=vmem,
        scratch_shapes=[
            pltpu.VMEM((ntp, count, part), BF16),
            pltpu.VMEM((count, features), BF16),
            pltpu.VMEM((3, n) + proj_state.shape, BF16),
            pltpu.VMEM((2, n) + merge_state.shape, BF16),
            pltpu.VMEM((count, width), BF16),
            pltpu.VMEM((count, 2 * lanes), F32),
            pltpu.VMEM((count, lanes), F32),
            pltpu.VMEM((count, 2 * lanes), BF16),
            pltpu.VMEM((count + BLOCK, width), F32),
            pltpu.VMEM((count, width), F32),
            pltpu.VMEM((count, width), BF16),
            pltpu.VMEM((count, width), BF16),
            pltpu.VMEM((BLOCK, width), BF16),
            pltpu.VMEM((BLOCK, width), BF16),
            pltpu.VMEM((8, lanes // 2), F32),
            pltpu.VMEM((n, 8, lanes // 2), F32),
            pltpu.VMEM((8, count), F32),
            pltpu.VMEM((ntp, 8, count), F32),
            pieces, pieces, pieces, pieces, pieces,
            dma((6,)), dma((ny,)), dma((ny,)), dma((ny,)), dma((ny,)),
            dma((5, 2, hops)), dma((5, 2, hops)), dma, dma,
            dma((n,)), dma((n,)), dma((ntp,)), dma((ntp,)),
            dma((ny, quarters)), dma((ny, quarters)), dma((ny, quarters)), dma((ny, quarters)),
        ],
        compiler_params=pltpu.CompilerParams(
            collective_id=0, has_side_effects=True, vmem_limit_bytes=60 * 1024 * 1024
        ),
        name="mixer",
    )(
        tokens, norm_gain.reshape(1, features), proj_state, proj_value, proj_gate,
        decay_shift.T, expand, counts * base, jnp.cos(angle), jnp.sin(angle), binp, cout,
        skip_gain.reshape(1, width), init_state.reshape(2, lanes), conv_taps,
        channel_gain.reshape(1, width), merge_state, merge_conv,
    )


def per_device_any(n, ntp, *args):
    tokens, merge_state = args[0], args[15]
    fits = (
        n % 8 == 0 and ntp % 2 == 0 and args[2].shape[0] % 128 == 0 and merge_state.shape[1] % 128 == 0
        and tokens.shape[0] % 128 == 0 and args[5].size % 256 == 0 and args[13].shape[0] <= BLOCK
    )
    if fits:
        return fused(n, ntp, *args)
    return per_device(*args)


def solution(mesh):
    return jax.shard_map(
        functools.partial(per_device_any, mesh.shape["sp"], mesh.shape["tp"]),
        mesh=mesh,
        in_specs=(
            P("sp", "tp"),
            P(),
            P("sp", "tp"),
            P("sp", "tp"),
            P("sp", "tp"),
            P("tp", None),
            P("tp", None),
            P("tp"),
            P("tp", "sp"),
            P(None, "tp", None, None),
            P(None, "tp", None, None),
            P("tp"),
            P(None, "tp", None),
            P(None, "tp"),
            P("tp"),
            P("tp", "sp"),
            P("tp", "sp"),
        ),
        out_specs=P(("sp", "tp"), None),
        check_vma=False,
    )
```

profile of v0, /device:TPU:0, one launch (start us, length us, event | category | flops | bytes accessed | tf_op | source)
XLA Modules:
  0.0 99.2 jit_solution(5384142426539900129)
XLA Ops:
  0.0 0.7 exp.6
  0.7 0.8 fusion.6
  1.5 1.0 fusion.10
  2.5 0.1 copy.19
  2.6 0.1 copy.20
  2.7 0.9 slice.15
  3.6 0.1 copy.22
  3.7 0.3 fusion.2
  4.0 0.1 pad_maximum_fusion
  4.2 1.9 %copy.23.binp = f32[256,2048]{1,0:T(8,128)} copy(f32[256,2048]{0,1:T(8,128)S(1)} %pad_maximum_fusion) | data formatting | bytes 4194304 | tf_op jit(solution)/shard_map/concatenate | solution.py:669
  6.0 0.0 copy-start
  6.0 0.0 copy-start.1
  6.0 0.9 slice.14
  7.0 0.1 copy.21
  7.1 0.2 fusion
  7.3 1.1 %maximum_bitcast_fusion.cout = bf16[2048,256]{1,0:T(8,128)(2,1)} fusion(bf16[256,1024]{0,1:T(8,128)(2,1)S(1)} %get-tuple-element.13, bf16[256,1024]{0,1:T(8,128)(2,1)S(1)} %fusion), kind=kLoop, calls=%fused_computation.8 | loop fusion | flops 2097152 | bytes 2097152 | tf_op jit(solution)/shard_map/transpose | solution.py:672
  8.3 0.1 mul.127
  8.4 0.1 mul.131
  8.5 1.3 %multiply_sine_fusion = (f32[32,1024]{1,0:T(8,128)}, f32[32,1024]{1,0:T(8,128)}, f32[32,1024]{1,0:T(8,128)}) fusion(f32[1024]{0:T(1024)S(1)} %mul.131, f32[32]{0:T(128)S(1)} %add_convert_fusion, f32[1024]{0:T(1024)S(1)} %mul.127), kind=kLoop, calls=%fused_computation.13 | loop fusion | flops 65536 | bytes 401536 | tf_op jit(solution)/shard_map/sin | solution.py:718
  9.8 0.6 fusion.5.expand
  10.4 0.0 copy-done
  10.4 0.8 copy.18
  11.3 0.0 copy-done.1
  11.3 0.7 reshape.160.init
  11.9 85.4 %mixer.1 = bf16[128,2048]{1,0:T(8,128)(2,1)} custom-call(bf16[512,512]{1,0:T(8,128)(2,1)} %tokens.1, f32[1,2048]{1,0:T(1,128)} %bitcast.39, bf16[256,256]{1,0:T(8,128)(2,1)} %proj_s.1, bf16[256,256]{1,0:T(8,128)(2,1)} %proj_v.1, bf16[256,256]{1,0:T(8,128)(2,1)} %proj_g.1, f32[512,16]{1,0:T(8,128)} %bitcast.36, f32[16,1024]{1,0:T(8,128)} %fusion.5.expand, ...), custom_call_target="tpu_custom_call" | custom-call | tf_op jit(solution)/shard_map/mixer/pallas_call | solution.py:682
  97.3 1.9 %copy.25 = bf16[128,2048]{1,0:T(8,128)(2,1)} copy(bf16[128,2048]{1,0:T(8,128)(2,1)} %mixer.1) | data formatting | bytes 1048576
  (4 shorter events, 0.0 us)
Async XLA Ops:
  6.0 4.4 %copy-start = (f32[16,512]{1,0:T(8,128)S(1)}, f32[16,512]{1,0:T(8,128)}, u32[]{:S(2)}) copy-start(f32[16,512]{1,0:T(8,128)} %param.25) | copy-start | bytes 98308
  6.0 5.2 %copy-start.1 = (f32[2,16,64]{2,1,0:T(8,128)S(1)}, f32[2,16,64]{2,1,0:T(8,128)}, u32[]{:S(2)}) copy-start(f32[2,16,64]{2,1,0:T(8,128)} %param.29) | copy-start | bytes 24580
where the time goes:
time: 99.9 us; the launch traced here: 99.2 us
  Pallas kernels  85.4 us (85%)
  local copies, waits for them, and re-layouts  9.22 us (9%)
  other arithmetic  4.51 us (5%)
    pallas_call x1, Pallas kernels, fused(): pl.pallas_call(functools.partial(mixer_kernel, n, ntp), out_shape=jax.Sha...  85.4 us
    unnamed x6, local copies, waits for them, and re-layouts  2.72 us

commit v1 on v0

--- a/solution.py
+++ b/solution.py
@@ -291,10 +291,11 @@
 
 def mixer_kernel(
     n, ntp,
-    tokens, gain, proj_s, proj_v, proj_g, shift, expand, base_t, cos_t, sin_t,
-    binp, cout, skip, init, taps, chgain, merge_s, merge_c,
+    tokens, gain, proj_s, proj_v, proj_g, eig_re, eig_im, log_step, decay,
+    state_in, state_out, skip, init, taps, chgain, merge_s, merge_c,
     out,
-    tok, normed, gat, mgat, u_buf, forc, grow_buf, xs, ext, raw, ssm, conv,
+    shift, base_t, cos_t, sin_t, bin_high, bin_low, cout, into_re, into_im, back_re, back_im, held,
+    tok, normed, gat, mgat, u_buf, forc, xs, ext, raw, ssm, conv,
     halo, glu_tail, summ, summ_in, stat, stat_in, snd, own, rp, s2, r2,
     loc_sem, tok_s, tok_r, fwd_s, fwd_r, ring_s, ring_r, halo_s, halo_r,
     sum_s, sum_r, st_s, st_r, rp_s, rp_r, r2_s, r2_r,
@@ -307,7 +308,8 @@
     pos = ring_position(sp, n)
     right, left = ring_index(pos + 1, n), ring_index(pos - 1, n)
     count, width = u_buf.shape
-    lanes = grow_buf.shape[1]
+    groups, states = eig_re.shape
+    lanes = groups * states
     part = tokens.shape[1]
     rows_w = proj_s.shape[0]
 
@@ -355,8 +357,7 @@
             for side in range(2):
                 piece(w, side, hops - 1).wait_recv()
 
-    proj_set, merge_set = range(3), range(3, 5)
-    ring_send(proj_set, 0)
+    ring_send([0, 1], 0)
 
     def tok_copy(d):
         where = (sp, lax.rem(y + d, ny) * 2 + core) if d else (sp, partner)
@@ -373,15 +374,97 @@
         local.append(pltpu.make_async_copy(sources[w], slot(w, sp), loc_sem.at[w]))
     for c in local:
         c.start()
-    ring_send(proj_set, 1)
+
+    row_i = lax.broadcasted_iota(jnp.int32, (BLOCK, BLOCK), 0)
+    col_i = lax.broadcasted_iota(jnp.int32, (BLOCK, BLOCK), 1)
+    lower = (row_i >= col_i).astype(F32)
+    last = slice(BLOCK - 1, BLOCK)
+
+    def lane_of(rows):
+        return lax.broadcasted_iota(jnp.int32, (rows, lanes), 1)
+
+    def row_of(rows):
+        return lax.broadcasted_iota(jnp.int32, (rows, lanes), 0)
+
+    repeat = (lax.rem(lane_of(states), states) == row_of(states)).astype(F32)
+    mine = lax.div(lane_of(groups), states) == row_of(groups)
+    expand = mine.astype(F32)
+
+    def to_row(matrix):
+        return jnp.sum(jnp.where(mine, dot_exact(matrix, repeat), 0.0), axis=0, keepdims=True)
+
+    square_row = lax.broadcasted_iota(jnp.int32, (groups, groups), 0)
+    square_col = lax.broadcasted_iota(jnp.int32, (groups, groups), 1)
+    steps = jnp.broadcast_to(jnp.exp(log_step[...]), (groups, groups))
+    step_size = jnp.sum(jnp.where(square_row == square_col, steps, 0.0), axis=1, keepdims=True)
+    real_row, imag_row = to_row(eig_re[...]), to_row(eig_im[...])
+    base_row = to_row(eig_re[...] * step_size)
+    theta_row = to_row(eig_im[...] * step_size)
+    counts = (row_of(BLOCK) + 1).astype(F32)
+    base_t[...] = counts * base_row
+    cos_t[...] = jnp.cos(counts * theta_row)
+    sin_t[...] = jnp.sin(counts * theta_row)
+    magnitude = jnp.exp(base_row)
+    near_re = magnitude * cos_t[0:1, :] - 1.0
+    near_im = magnitude * sin_t[0:1, :]
+    modulus = real_row * real_row + imag_row * imag_row
+    ratio_re = (near_re * real_row + near_im * imag_row) / modulus
+    ratio_im = (near_im * real_row - near_re * imag_row) / modulus
+    group = width // groups
+    chunk = 256
+    for j in range(lanes // chunk):
+        cols = slice(j * chunk, (j + 1) * chunk)
+        later = slice(lanes + j * chunk, lanes + (j + 1) * chunk)
+        spot = lax.broadcasted_iota(jnp.int32, (width, chunk), 1) + j * chunk
+        whose = lax.div(lax.broadcasted_iota(jnp.int32, (width, chunk), 0), group)
+        same = lax.div(spot, states) == whose
+        m_re = dot_exact(state_in[0:width, :], repeat[:, cols])
+        m_im = dot_exact(state_in[width : 2 * width, :], repeat[:, cols])
+        r_re, r_im = ratio_re[:, cols], ratio_im[:, cols]
+        bin_high[:, cols], bin_low[:, cols] = split(jnp.where(same, r_re * m_re - r_im * m_im, 0.0))
+        bin_high[:, later], bin_low[:, later] = split(jnp.where(same, r_re * m_im + r_im * m_re, 0.0))
+        m_re = dot_exact(state_out[0:width, :], repeat[:, cols])
+        m_im = dot_exact(state_out[width : 2 * width, :], repeat[:, cols])
+        cout[:, cols] = jnp.where(same, m_re, 0.0).astype(BF16)
+        cout[:, later] = jnp.where(same, -m_im, 0.0).astype(BF16)
+    start_re, start_im = to_row(init[0:groups, :]), to_row(init[groups : 2 * groups, :])
+    fill_rows = jnp.zeros((128 - groups, count), F32)
+    shift[...] = jnp.concatenate([decay[...], fill_rows], axis=0).T
+
+    ring_send([0, 1], 1)
+
+    def prepare(k, state):
+        a_re, a_im = state
+        rows = pl.ds(pl.multiple_of(k * BLOCK, BLOCK), BLOCK)
+        level = dot_exact(dot_exact(lower, shift[rows, :])[:, :groups], expand) + base_t[...]
+        grow, shrink = jnp.exp(level), jnp.exp(-level)
+        cosine, sine = cos_t[...], sin_t[...]
+        into_re[rows, :] = shrink * cosine
+        into_im[rows, :] = shrink * sine
+        g_re, g_im = grow * cosine, grow * sine
+        back_re[rows, :] = g_re
+        back_im[rows, :] = g_im
+        held[0, pl.ds(k, 1), :] = a_re
+        held[1, pl.ds(k, 1), :] = a_im
+        e_re, e_im = g_re[last], g_im[last]
+        return a_re * e_re - a_im * e_im, a_re * e_im + a_im * e_re
+
+    zero = jnp.zeros((1, lanes), F32)
+    blocks = count // BLOCK
+    decayed = lax.fori_loop(0, blocks // 2, prepare, (zero + 1.0, zero))
+    ring_send([0, 1], 2)
     for d in range(1, ny):
         tok_copy(d).wait_recv()
         tok_forward(d).start()
+    decayed = lax.fori_loop(blocks // 2, blocks, prepare, decayed)
+    for step in range(3, hops - 1):
+        ring_send([0, 1], step)
+    ring_send([0], hops - 1)
+    ring_send([2], 0)
+    ring_send([1], hops - 1)
     tok_copy(0).wait_recv()
     for c in local:
         c.wait()
-    for step in range(2, hops - 1):
-        ring_send(proj_set, step)
     for d in range(1, ny):
         tok_forward(d).wait_recv()
 
@@ -397,9 +480,7 @@
             cols = slice(j * part, (j + 1) * part)
             normed[rows, cols] = (pieces[j] * scale * gain[:, cols]).astype(BF16)
 
-    ring_send(proj_set, hops - 1)
-    ring_send(merge_set, 0)
-    ring_end(proj_set)
+    ring_end([0])
 
     big = 128
 
@@ -412,14 +493,105 @@
 
     @pl.loop(0, count // big)
     def _(i):
+        rows, u = project(0, i)
+        u_buf[rows, :] = u
+
+    wide = 256
+
+    @pl.loop(0, 2 * lanes // wide)
+    def _(j):
+        cols = pl.ds(pl.multiple_of(j * wide, wide), wide)
+        forc[:, cols] = dot(u_buf[...], bin_high[:, cols]) + dot(u_buf[...], bin_low[:, cols])
+
+    ring_send([3], 0)
+    ring_send([2], 1)
+
+    def first_pass(k, state):
+        c_re, c_im = state
+        rows = pl.ds(pl.multiple_of(k * BLOCK, BLOCK), BLOCK)
+        held[2, pl.ds(k, 1), :] = c_re
+        held[3, pl.ds(k, 1), :] = c_im
+        d_re, d_im = forc[rows, :lanes], forc[rows, lanes:]
+        w_re = into_re[rows, :] * d_re + into_im[rows, :] * d_im
+        w_im = into_re[rows, :] * d_im - into_im[rows, :] * d_re
+        forc[rows, :lanes] = w_re
+        forc[rows, lanes:] = w_im
+        final = pl.ds(k * BLOCK + BLOCK - 1, 1)
+        e_re, e_im = back_re[final, :], back_im[final, :]
+        t_re = c_re + jnp.sum(w_re, axis=0, keepdims=True)
+        t_im = c_im + jnp.sum(w_im, axis=0, keepdims=True)
+        return e_re * t_re - e_im * t_im, e_re * t_im + e_im * t_re
+
+    ended = decayed + lax.fori_loop(0, blocks, first_pass, (zero, zero))
+    half = lanes // 2
+    for r in range(4):
+        summ[r : r + 1, :] = ended[r][:, :half]
+        summ[4 + r : 5 + r, :] = ended[r][:, half:]
+
+    def summ_copy(d):
+        return remote(summ, summ_in.at[sp], sum_s.at[d], sum_r.at[d], (lax.rem(sp + d, n), tp))
+
+    for d in range(1, n):
+
+        @pl.when(sp + d < n)
+        def _():
+            summ_copy(d).start()
+
+    ring_send([4], 0)
+    ring_send([2], 2)
+
+
+    for d in range(1, n):
+
+        @pl.when(sp >= d)
+        def _():
+            summ_copy(d).wait_recv()
+
+    def unpack(block):
+        return [jnp.concatenate([block[r : r + 1], block[4 + r : 5 + r]], axis=1) for r in range(4)]
+
+    h_re, h_im = start_re, start_im
+    for q in range(n - 1):
+        a_re, a_im, b_re, b_im = unpack(summ_in[q])
+        n_re = a_re * h_re - a_im * h_im + b_re
+        n_im = a_re * h_im + a_im * h_re + b_im
+        h_re = jnp.where(q < sp, n_re, h_re)
+        h_im = jnp.where(q < sp, n_im, h_im)
+
+    lower_half = lower.astype(BF16)
+
+    def second_pass(k, _):
+        rows = pl.ds(pl.multiple_of(k * BLOCK, BLOCK), BLOCK)
+        one = pl.ds(k, 1)
+        a_re, a_im = held[0, one, :], held[1, one, :]
+        c_re = held[2, one, :] + a_re * h_re - a_im * h_im
+        c_im = held[3, one, :] + a_re * h_im + a_im * h_re
+        high, low = split(forc[rows, :])
+        summed = dot(lower_half, high) + dot(lower_half, low)
+        t_re = summed[:, :lanes] + c_re
+        t_im = summed[:, lanes:] + c_im
+        g_re, g_im = back_re[rows, :], back_im[rows, :]
+        xs[rows, :lanes] = (g_re * t_re - g_im * t_im).astype(BF16)
+        xs[rows, lanes:] = (g_re * t_im + g_im * t_re).astype(BF16)
+        return 0
+
+    lax.fori_loop(0, blocks, second_pass, 0)
+    ring_send([3], 1)
+    for step in range(3, hops - 1):
+        ring_send([2], step)
+    ring_send([2], hops - 1)
+    ring_send([4], 1)
+    for step in range(2, hops - 2):
+        ring_send([3, 4], step)
+    ring_end([1, 2])
+
+    @pl.loop(0, count // big)
+    def _(i):
         rows, value = project(1, i)
         rows, gate = project(2, i)
         glu = (value.astype(F32) * jax.nn.sigmoid(gate.astype(F32))).astype(BF16)
         ext[pl.ds(pl.multiple_of(BLOCK + i * big, BLOCK), big), :] = glu.astype(F32)
-        rows, u = project(0, i)
-        u_buf[rows, :] = u
-
-    ring_send(merge_set, 1)
+
     glu_tail[...] = ext[count : count + BLOCK, :].astype(BF16)
     halo_to = lax.rem(sp + 1, n)
     halo_copy = remote(glu_tail, halo, halo_s, halo_r, (halo_to, tp))
@@ -428,69 +600,10 @@
     def _():
         halo_copy.start()
 
-    wide = 256
-
-    @pl.loop(0, 2 * lanes // wide)
-    def _(j):
-        cols = pl.ds(pl.multiple_of(j * wide, wide), wide)
-        high, low = split(binp[:, cols])
-        forc[:, cols] = dot(u_buf[...], high) + dot(u_buf[...], low)
-
-    row_i = lax.broadcasted_iota(jnp.int32, (BLOCK, BLOCK), 0)
-    col_i = lax.broadcasted_iota(jnp.int32, (BLOCK, BLOCK), 1)
-    lower = (row_i >= col_i).astype(F32)
-    last = slice(BLOCK - 1, BLOCK)
-
-    def first_pass(k, state):
-        a_re, a_im, c_re, c_im = state
-        rows = pl.ds(pl.multiple_of(k * BLOCK, BLOCK), BLOCK)
-        level = dot_exact(dot_exact(lower, shift[rows, :]), expand[...]) + base_t[...]
-        grow, shrink = jnp.exp(level), jnp.exp(-level)
-        cosine, sine = cos_t[...], sin_t[...]
-        d_re, d_im = forc[rows, :lanes], forc[rows, lanes:]
-        w_re = shrink * (cosine * d_re + sine * d_im)
-        w_im = shrink * (cosine * d_im - sine * d_re)
-        forc[rows, :lanes] = w_re
-        forc[rows, lanes:] = w_im
-        grow_buf[rows, :] = grow
-        e_re, e_im = grow[last] * cosine[last], grow[last] * sine[last]
-        t_re = c_re + jnp.sum(w_re, axis=0, keepdims=True)
-        t_im = c_im + jnp.sum(w_im, axis=0, keepdims=True)
-        return (
-            a_re * e_re - a_im * e_im,
-            a_re * e_im + a_im * e_re,
-            e_re * t_re - e_im * t_im,
-            e_re * t_im + e_im * t_re,
-        )
-
-    zero = jnp.zeros((1, lanes), F32)
-    ended = lax.fori_loop(0, count // BLOCK, first_pass, (zero + 1.0, zero, zero, zero))
-    half = lanes // 2
-    for r in range(4):
-        summ[r : r + 1, :] = ended[r][:, :half]
-        summ[4 + r : 5 + r, :] = ended[r][:, half:]
-
-    def summ_copy(d):
-        return remote(summ, summ_in.at[sp], sum_s.at[d], sum_r.at[d], (lax.rem(sp + d, n), tp))
-
-    for d in range(1, n):
-
-        @pl.when(sp + d < n)
-        def _():
-            summ_copy(d).start()
-
-    ring_send(merge_set, 2) if hops > 2 else None
-
-    @pl.when(sp > 0)
-    def _():
-        halo_copy.wait_recv()
-
-    ext[0:BLOCK, :] = halo[...].astype(F32)
     reach = taps.shape[0] - 1
-
-    @pl.loop(0, count // tile)
-    def _(i):
-        start = pl.multiple_of(i * tile, tile)
+    ring_send([3, 4], hops - 2)
+
+    def taps_on(start):
         window = ext[pl.ds(start, tile + BLOCK), :]
         total = jnp.zeros((tile, width), F32)
         for k in range(reach + 1):
@@ -498,6 +611,17 @@
             total += taps[k : k + 1, :] * window[at : at + tile, :]
         raw[pl.ds(start, tile), :] = total
 
+    @pl.loop(1, count // tile)
+    def _(i):
+        taps_on(pl.multiple_of(i * tile, tile))
+
+    @pl.when(sp > 0)
+    def _():
+        halo_copy.wait_recv()
+
+    ext[0:BLOCK, :] = halo[...].astype(F32)
+    taps_on(0)
+
     lane = lax.broadcasted_iota(jnp.int32, (count, 128), 1)
     values = raw[...]
     first = jnp.sum(values, axis=1, keepdims=True)
@@ -510,49 +634,14 @@
 
     for d in range(1, ntp):
         stat_copy(d).start()
-    for step in range(3, hops):
-        ring_send(merge_set, step)
-
-    for d in range(1, n):
-
-        @pl.when(sp >= d)
-        def _():
-            summ_copy(d).wait_recv()
-
-    def unpack(block):
-        return [jnp.concatenate([block[r : r + 1], block[4 + r : 5 + r]], axis=1) for r in range(4)]
-
-    h_re, h_im = init[0:1, :], init[1:2, :]
-    for q in range(n - 1):
-        a_re, a_im, b_re, b_im = unpack(summ_in[q])
-        n_re = a_re * h_re - a_im * h_im + b_re
-        n_im = a_re * h_im + a_im * h_re + b_im
-        h_re = jnp.where(q < sp, n_re, h_re)
-        h_im = jnp.where(q < sp, n_im, h_im)
-
-    lower_half = lower.astype(BF16)
-
-    def second_pass(k, state):
-        c_re, c_im = state
-        rows = pl.ds(pl.multiple_of(k * BLOCK, BLOCK), BLOCK)
-        high, low = split(forc[rows, :])
-        summed = dot(lower_half, high) + dot(lower_half, low)
-        t_re = summed[:, :lanes] + c_re
-        t_im = summed[:, lanes:] + c_im
-        grow = grow_buf[rows, :]
-        g_re, g_im = grow * cos_t[...], grow * sin_t[...]
-        x_re = g_re * t_re - g_im * t_im
-        x_im = g_re * t_im + g_im * t_re
-        xs[rows, :lanes] = x_re.astype(BF16)
-        xs[rows, lanes:] = x_im.astype(BF16)
-        return x_re[last], x_im[last]
-
-    lax.fori_loop(0, count // BLOCK, second_pass, (h_re, h_im))
+    ring_send([3, 4], hops - 1)
 
     @pl.loop(0, count // big)
     def _(i):
         rows = pl.ds(pl.multiple_of(i * big, big), big)
-        total = dot(xs[rows, :], cout[...])
+        total = lax.dot_general(
+            xs[rows, :], cout[...], (((1,), (1,)), ((), ())), preferred_element_type=F32
+        )
         total += skip[...] * u_buf[rows, :].astype(F32)
         ssm[rows, :] = jax.nn.gelu(total).astype(BF16)
 
@@ -569,7 +658,7 @@
     scaled = (raw[...] - columns[:, 0:1]) * columns[:, 1:2] * chgain[...]
     conv[...] = jax.nn.silu(scaled).astype(BF16)
 
-    ring_end(merge_set)
+    ring_end([3, 4])
     quarters, block_rows = snd.shape[1], snd.shape[2]
     per = n // quarters
     cw = merge_s.shape[1]
@@ -653,24 +742,6 @@
     width = proj_state.shape[1]
     lanes = groups * states
     features = part * ntp
-    step = jnp.exp(log_step)
-    base = (eigen_real * step[:, None]).reshape(1, lanes)
-    theta = (eigen_imag * step[:, None]).reshape(1, lanes)
-    counts = (jnp.arange(BLOCK) + 1).astype(F32)[:, None]
-    angle = counts * theta
-    b_re, b_im = input_matrix(eigen_real, eigen_imag, step, state_input)
-    group = width // groups
-    same = jnp.arange(width)[:, None] // group == jnp.arange(lanes)[None, :] // states
-
-    def spread_out(matrix):
-        tiled = jnp.tile(matrix.reshape(width, states), (1, groups))
-        return jnp.where(same, tiled, 0.0)
-
-    binp = jnp.concatenate([spread_out(b_re), spread_out(b_im)], axis=1)
-    cout = jnp.concatenate(
-        [spread_out(state_readout_matrices[0]), -spread_out(state_readout_matrices[1])], axis=1
-    ).astype(BF16).T
-    expand = (jnp.arange(groups)[:, None] == jnp.arange(lanes)[None, :] // states).astype(F32)
     quarters = min(4, n)
     ny = ntp // 2
     block_rows = count // ntp
@@ -682,16 +753,27 @@
     return pl.pallas_call(
         functools.partial(mixer_kernel, n, ntp),
         out_shape=jax.ShapeDtypeStruct((block_rows, features), BF16),
-        in_specs=[vmem] * 18,
+        in_specs=[vmem] * 17,
         out_specs=vmem,
         scratch_shapes=[
+            pltpu.VMEM((count, 128), F32),
+            pltpu.VMEM((BLOCK, lanes), F32),
+            pltpu.VMEM((BLOCK, lanes), F32),
+            pltpu.VMEM((BLOCK, lanes), F32),
+            pltpu.VMEM((width, 2 * lanes), BF16),
+            pltpu.VMEM((width, 2 * lanes), BF16),
+            pltpu.VMEM((width, 2 * lanes), BF16),
+            pltpu.VMEM((count, lanes), F32),
+            pltpu.VMEM((count, lanes), F32),
+            pltpu.VMEM((count, lanes), F32),
+            pltpu.VMEM((count, lanes), F32),
+            pltpu.VMEM((4, max(count // BLOCK, 8), lanes), F32),
             pltpu.VMEM((ntp, count, part), BF16),
             pltpu.VMEM((count, features), BF16),
             pltpu.VMEM((3, n) + proj_state.shape, BF16),
             pltpu.VMEM((2, n) + merge_state.shape, BF16),
             pltpu.VMEM((count, width), BF16),
             pltpu.VMEM((count, 2 * lanes), F32),
-            pltpu.VMEM((count, lanes), F32),
             pltpu.VMEM((count, 2 * lanes), BF16),
             pltpu.VMEM((count + BLOCK, width), F32),
             pltpu.VMEM((count, width), F32),
@@ -715,8 +797,9 @@
         name="mixer",
     )(
         tokens, norm_gain.reshape(1, features), proj_state, proj_value, proj_gate,
-        decay_shift.T, expand, counts * base, jnp.cos(angle), jnp.sin(angle), binp, cout,
-        skip_gain.reshape(1, width), init_state.reshape(2, lanes), conv_taps,
+        eigen_real, eigen_imag, log_step.reshape(1, groups), decay_shift,
+        state_input.reshape(2 * width, states), state_readout_matrices.reshape(2 * width, states),
+        skip_gain.reshape(1, width), init_state.reshape(2 * groups, states), conv_taps,
         channel_gain.reshape(1, width), merge_state, merge_conv,
     )
 

time: 99.9 us -> 84.2 us (0.84)
  local copies, waits for them, and re-layouts: 9.22 us -> 1.88 us
  other arithmetic: 4.51 us -> 0 us
  Pallas kernels: 85.4 us -> 82.2 us
    pallas_call x1, Pallas kernels: 85.4 us -> 82.2 us  [fused(): pl.pallas_call(functools.partial(mixer_kernel, n, ntp), out_shape=jax.Sha...]
    slice x3 -> x0, local copies, waits for them, and re-layouts: 2.83 us -> none  [the longest x1 0.99 us: input_matrix(): in_re = state_input[0]]
    concatenate x1 -> x0, local copies, waits for them, and re-layouts: 1.88 us -> none  [fused(): binp = jnp.concatenate([spread_out(b_re), spread_out(b_im)], axis=1)]
    sin x1 -> x0, other arithmetic: 1.29 us -> none  [fused(): jnp.sin(angle)]
    transpose x1 -> x0, other arithmetic: 1.07 us -> none  [fused(): cout = jnp.concatenate([spread_out(state_readout_matrices[0]), -spread_ou...]
    unnamed x6 -> x1, local copies, waits for them, and re-layouts: 2.72 us -> 1.88 us
where the time goes in v1:
time: 84.2 us; the launch traced here: 84 us
  Pallas kernels  82.2 us (98%)
  local copies, waits for them, and re-layouts  1.88 us (2%)
    pallas_call x1, Pallas kernels, fused(): pl.pallas_call(functools.partial(mixer_kernel, n, ntp), out_shape=jax.Sha...  82.2 us
    unnamed x1, local copies, waits for them, and re-layouts  1.88 us

profile of v1, /device:TPU:0, one launch (start us, length us, event | category | flops | bytes accessed | tf_op | source)
XLA Modules:
  0.0 84.0 jit_solution(11665283791892756257)
XLA Ops:
  0.0 82.2 %mixer.1 = bf16[128,2048]{1,0:T(8,128)(2,1)} custom-call(bf16[512,512]{1,0:T(8,128)(2,1)} %tokens.1, f32[1,2048]{1,0:T(1,128)} %bitcast.10, bf16[256,256]{1,0:T(8,128)(2,1)} %proj_s.1, bf16[256,256]{1,0:T(8,128)(2,1)} %proj_v.1, bf16[256,256]{1,0:T(8,128)(2,1)} %proj_g.1, f32[16,64]{1,0:T(8,128)} %eig_re.1, f32[16,64]{1,0:T(8,128)} %eig_im.1, ...), custom_call_target="tpu_custom_call" | custom-call | tf_op jit(solution)/shard_map/mixer/pallas_call | solution.py:753
  82.2 1.9 %copy.19 = bf16[128,2048]{1,0:T(8,128)(2,1)} copy(bf16[128,2048]{1,0:T(8,128)(2,1)} %mixer.1) | data formatting | bytes 1048576

commit v2 on v1

--- a/solution.py
+++ b/solution.py
@@ -462,6 +462,7 @@
     ring_send([0], hops - 1)
     ring_send([2], 0)
     ring_send([1], hops - 1)
+    ring_send([3], 0)
     tok_copy(0).wait_recv()
     for c in local:
         c.wait()
@@ -496,15 +497,15 @@
         rows, u = project(0, i)
         u_buf[rows, :] = u
 
+    ring_send([2], 1)
+    ring_send([4], 0)
+
     wide = 256
 
     @pl.loop(0, 2 * lanes // wide)
     def _(j):
         cols = pl.ds(pl.multiple_of(j * wide, wide), wide)
         forc[:, cols] = dot(u_buf[...], bin_high[:, cols]) + dot(u_buf[...], bin_low[:, cols])
-
-    ring_send([3], 0)
-    ring_send([2], 1)
 
     def first_pass(k, state):
         c_re, c_im = state
@@ -522,7 +523,10 @@
         t_im = c_im + jnp.sum(w_im, axis=0, keepdims=True)
         return e_re * t_re - e_im * t_im, e_re * t_im + e_im * t_re
 
-    ended = decayed + lax.fori_loop(0, blocks, first_pass, (zero, zero))
+    ended = lax.fori_loop(0, blocks // 2, first_pass, (zero, zero), unroll=2)
+    ring_send([2], 2)
+    ring_send([3], 1)
+    ended = decayed + lax.fori_loop(blocks // 2, blocks, first_pass, ended, unroll=2)
     half = lanes // 2
     for r in range(4):
         summ[r : r + 1, :] = ended[r][:, :half]
@@ -536,9 +540,6 @@
         @pl.when(sp + d < n)
         def _():
             summ_copy(d).start()
-
-    ring_send([4], 0)
-    ring_send([2], 2)
 
 
     for d in range(1, n):
@@ -575,14 +576,13 @@
         xs[rows, lanes:] = (g_re * t_im + g_im * t_re).astype(BF16)
         return 0
 
-    lax.fori_loop(0, blocks, second_pass, 0)
-    ring_send([3], 1)
+    lax.fori_loop(0, blocks // 2, second_pass, 0, unroll=2)
     for step in range(3, hops - 1):
         ring_send([2], step)
     ring_send([2], hops - 1)
     ring_send([4], 1)
-    for step in range(2, hops - 2):
-        ring_send([3, 4], step)
+    lax.fori_loop(blocks // 2, blocks, second_pass, 0, unroll=2)
+    ring_send([3], 2)
     ring_end([1, 2])
 
     @pl.loop(0, count // big)
@@ -601,7 +601,9 @@
         halo_copy.start()
 
     reach = taps.shape[0] - 1
-    ring_send([3, 4], hops - 2)
+    ring_send([4], 2)
+    for step in range(3, hops - 1):
+        ring_send([3, 4], step)
 
     def taps_on(start):
         window = ext[pl.ds(start, tile + BLOCK), :]

time: 84.2 us -> 83.1 us (0.987)
  Pallas kernels: 82.2 us -> 81.1 us
    pallas_call x1, Pallas kernels: 82.2 us -> 81.1 us  [fused(): pl.pallas_call(functools.partial(mixer_kernel, n, ntp), out_shape=jax.Sha...]
where the time goes in v2:
time: 83.1 us; the launch traced here: 83 us
  Pallas kernels  81.1 us (98%)
  local copies, waits for them, and re-layouts  1.88 us (2%)
    pallas_call x1, Pallas kernels, fused(): pl.pallas_call(functools.partial(mixer_kernel, n, ntp), out_shape=jax.Sha...  81.1 us
    unnamed x1, local copies, waits for them, and re-layouts  1.88 us

profile of v2, /device:TPU:0, one launch (start us, length us, event | category | flops | bytes accessed | tf_op | source)
XLA Modules:
  0.0 83.0 jit_solution(12885631046502100400)
XLA Ops:
  0.0 81.1 %mixer.1 = bf16[128,2048]{1,0:T(8,128)(2,1)} custom-call(bf16[512,512]{1,0:T(8,128)(2,1)} %tokens.1, f32[1,2048]{1,0:T(1,128)} %bitcast.10, bf16[256,256]{1,0:T(8,128)(2,1)} %proj_s.1, bf16[256,256]{1,0:T(8,128)(2,1)} %proj_v.1, bf16[256,256]{1,0:T(8,128)(2,1)} %proj_g.1, f32[16,64]{1,0:T(8,128)} %eig_re.1, f32[16,64]{1,0:T(8,128)} %eig_im.1, ...), custom_call_target="tpu_custom_call" | custom-call | tf_op jit(solution)/shard_map/mixer/pallas_call | solution.py:755
  81.1 1.9 %copy.19 = bf16[128,2048]{1,0:T(8,128)(2,1)} copy(bf16[128,2048]{1,0:T(8,128)(2,1)} %mixer.1) | data formatting | bytes 1048576
